TPU v7x, 32 devices: a whole 2x2x4 slice. The times are simulated.
32 devices in a mesh: sp: 8 (over z, x), tp: 4 (over y, core).
Axes of the slice: x: 2, y: 2, z: 4, core: 2. Of those that a mesh axis runs over, the one named last changes fastest.
Arguments:
- residual_in: bfloat16 [2048, 2048], P(('sp', 'tp')), may hold values from -0.119628906 to 0.119628906
- queries: bfloat16 [2048, 2048], P('sp', 'tp'), may hold values from -6 to 6
- keys_raw: bfloat16 [2048, 512], P('sp', 'tp'), may hold values from -6 to 6
- values_raw: bfloat16 [2048, 512], P('sp', 'tp'), may hold values from -6 to 6
- query_gain: float32 [128], replicated, may hold values from 0.28 to 7
- key_gain: float32 [128], replicated, may hold values from 0.28 to 7
- out_weight: bfloat16 [2048, 2048], P('tp'), may hold values from -0.125 to 0.125
- norm_gain: float32 [2048], replicated, may hold values from 0.1 to 1.9
- gate_weight: bfloat16 [2048, 5632], P('sp', 'tp'), may hold values from -0.125 to 0.125
- up_weight: bfloat16 [2048, 5632], P('sp', 'tp'), may hold values from -0.125 to 0.125
- down_weight: bfloat16 [5632, 2048], P('tp', 'sp'), may hold values from -0.078125 to 0.078125
Outputs:
- residual_out: bfloat16 [2048, 2048], P(('sp', 'tp'))
All inputs are finite; a program needn't handle non-finite values.
Results may differ from a plain program's by a relative error of at most 0.024.
The roundings to bfloat16 on the way count: a program that leaves them out, or rounds other values in their place, can miss the bound.
Values may be sent and summed in bfloat16 or wider, within the bound.
A program may use at most 128 MiB of HBM per device.

v0:
```python
import jax
import jax.numpy as jnp
from jax import lax
from jax.sharding import PartitionSpec as P

GRID_W = 64
EPS = 1e-06
THETA = 10000.0


def turn_half(part, angles):
    quarter = part.shape[-1] // 2
    cosine = jnp.cos(angles)[:, None, :]
    sine = jnp.sin(angles)[:, None, :]
    first = part[..., :quarter]
    second = part[..., quarter:]
    return part * cosine + jnp.concatenate([-second, first], axis=-1) * sine


def prepare_heads(raw, gain, positions, heads):
    count = raw.shape[0]
    head_dim = gain.shape[0]
    half = head_dim // 2
    vec = raw.astype(jnp.float32).reshape(count, heads, head_dim)
    vec = vec * lax.rsqrt(jnp.mean(vec * vec, axis=-1, keepdims=True) + EPS) * gain
    freqs = THETA ** (-jnp.arange(0, half, 2, dtype=jnp.float32) / half)
    row_ang = (positions // GRID_W).astype(jnp.float32)[:, None] * freqs
    col_ang = (positions % GRID_W).astype(jnp.float32)[:, None] * freqs
    row_ang = jnp.concatenate([row_ang, row_ang], axis=-1)
    col_ang = jnp.concatenate([col_ang, col_ang], axis=-1)
    turned = jnp.concatenate(
        [turn_half(vec[..., :half], row_ang), turn_half(vec[..., half:], col_ang)], axis=-1
    )
    return turned.astype(jnp.bfloat16)


def per_device(
    residual_in,
    queries,
    keys_raw,
    values_raw,
    query_gain,
    key_gain,
    out_weight,
    norm_gain,
    gate_weight,
    up_weight,
    down_weight,
):
    tok = queries.shape[0]
    head_dim = query_gain.shape[0]
    local_heads = queries.shape[1] // head_dim
    local_kv = keys_raw.shape[1] // head_dim
    group = local_heads // local_kv
    gate_full, up_full = (
        lax.all_gather(gate_weight, "sp", axis=0, tiled=True),
        lax.all_gather(up_weight, "sp", axis=0, tiled=True),
    )
    down_full = lax.all_gather(down_weight, "sp", axis=1, tiled=True)
    positions = lax.axis_index("sp") * tok + jnp.arange(tok, dtype=jnp.int32)
    q_rot = prepare_heads(queries, query_gain, positions, local_heads).reshape(
        tok, local_kv, group, head_dim
    )
    k_rot = prepare_heads(keys_raw, key_gain, positions, local_kv)
    vals = values_raw.reshape(tok, local_kv, head_dim)
    start_state = (
        jnp.full((tok, local_kv, group), -jnp.inf, jnp.float32),
        jnp.zeros((tok, local_kv, group), jnp.float32),
        jnp.zeros((tok, local_kv, group, head_dim), jnp.float32),
    )
    carry = start_state
    k_piece = lax.all_gather(k_rot, "sp", axis=0, tiled=True)
    v_piece = lax.all_gather(vals, "sp", axis=0, tiled=True)
    length = k_piece.shape[0]
    shards = length // tok
    per_step = max(1, 2048 // tok)
    factor = max((d for d in range(1, shards + 1) if shards % d == 0 and d <= per_step))
    span = factor * tok
    k_blocks = k_piece.reshape(length // span, span, local_kv, head_dim)
    v_blocks = v_piece.reshape(length // span, span, local_kv, head_dim)

    def step(state, blocks):
        top, total, summed = state
        k_blk, v_blk = blocks
        scores = jnp.einsum(
            "qkgd,skd->qkgs", q_rot, k_blk, preferred_element_type=jnp.float32
        ) * head_dim ** (-0.5)
        new_top = jnp.maximum(top, jnp.max(scores, axis=-1))
        shrink = jnp.exp(top - new_top)
        expo = jnp.exp(scores - new_top[..., None])
        total = total * shrink + jnp.sum(expo, axis=-1)
        summed = summed * shrink[..., None] + jnp.einsum(
            "qkgs,skd->qkgd", expo.astype(jnp.bfloat16), v_blk, preferred_element_type=jnp.float32
        )
        return ((new_top, total, summed), None)

    carry, _ = lax.scan(step, carry, (k_blocks, v_blocks))
    top, total, summed = carry
    attended = (summed / total[..., None]).astype(jnp.bfloat16).reshape(tok, local_heads * head_dim)
    projected = lax.psum_scatter(
        jnp.dot(attended, out_weight, preferred_element_type=jnp.float32).astype(jnp.bfloat16),
        "tp",
        scatter_dimension=0,
        tiled=True,
    ).astype(jnp.float32)
    mixed = (residual_in.astype(jnp.float32) + projected).astype(jnp.bfloat16)
    mixed_f = mixed.astype(jnp.float32)
    normed = (
        mixed_f * lax.rsqrt(jnp.mean(mixed_f * mixed_f, axis=-1, keepdims=True) + EPS) * norm_gain
    ).astype(jnp.bfloat16)
    whole_rows = lax.all_gather(normed, "tp", axis=0, tiled=True)
    gate = jnp.dot(whole_rows, gate_full, preferred_element_type=jnp.float32)
    up_val = jnp.dot(whole_rows, up_full, preferred_element_type=jnp.float32)
    hidden = (jax.nn.silu(gate) * up_val).astype(jnp.bfloat16)
    terms = jnp.dot(hidden, down_full, preferred_element_type=jnp.float32)
    fed = lax.psum_scatter(
        terms.astype(jnp.bfloat16), "tp", scatter_dimension=0, tiled=True
    ).astype(jnp.float32)
    return (mixed_f + 0.5 * fed).astype(jnp.bfloat16)


def solution(mesh):
    placed = (
        P(("sp", "tp"), None),
        P("sp", "tp"),
        P("sp", "tp"),
        P("sp", "tp"),
        P(),
        P(),
        P("tp", None),
        P(),
        P("sp", "tp"),
        P("sp", "tp"),
        P("tp", "sp"),
    )
    return jax.shard_map(
        per_device, mesh=mesh, in_specs=placed, out_specs=P(("sp", "tp"), None), check_vma=False
    )
```

profile of v0, /device:TPU:0, one launch (start us, length us, event | category | flops | bytes accessed | tf_op | source)
XLA Modules:
  0.0 460.9 jit_solution(13443270139341550448)
XLA Ops:
  6.6 1.1 fusion.33
  7.7 0.9 fusion.35
  8.8 0.8 broadcast_multiply_fusion.1
  9.6 1.2 fusion.39
  10.9 33.0 %all_gather.18 = bf16[2048,1,128]{2,0,1:T(8,128)(2,1)S(1)} all-gather(bf16[256,1,128]{2,0,1:T(8,128)(2,1)S(1)} %pad_maximum_fusion.4), channel_id=1, replica_groups=mesh['sp'=8,'tp'=4] {'sp'}, dimensions={0}, use_global_device_ids=true | all-gather | bytes 589824 | tf_op jit(solution)/shard_map/all_gather | solution.py:72
  43.9 1.1 copy.14
  45.2 0.9 multiply_multiply_fusion
  46.1 0.5 slice_negate_fusion.1
  46.6 1.5 fusion.43
  48.1 0.5 fusion.41
  48.7 0.5 fusion.26
  49.1 1.3 bitcast_reduce_fusion
  50.5 3.2 copy-done.1
  53.7 1.4 fusion.1
  55.2 31.3 %all-gather = bf16[2048,128]{0,1:T(8,128)(2,1)S(1)} all-gather(bf16[256,128]{0,1:T(8,128)(2,1)S(1)} %copy.16), channel_id=2, replica_groups=mesh['sp'=8,'tp'=4] {'sp'}, dimensions={0}, use_global_device_ids=true | all-gather | bytes 589824 | tf_op jit(solution)/shard_map/all_gather | solution.py:73
  86.5 5.1 %fusion.16 = bf16[1,128,256,4]{2,1,3,0:T(8,128)(2,1)S(1)} fusion(f32[2048,256,4]{1,0,2:T(8,128)} %copy-done.1, f32[256,4]{0,1:T(4,128)S(1)} %get-tuple-element.50, bf16[2048,128]{0,1:T(8,128)(2,1)S(1)} %all-gather, f32[256,4]{0,1:T(4,128)S(1)} %get-tuple-element.43, f32[256,4]{0,1:T(4,128)S(1)} %get-tuple-element.42), kind=kOutput, calls=%fused_computation.14 | convolution fusion | flops 543555584 | bytes 9187328 | tf_op jit(solution)/shard_map/while/body/eval_jaxpr/qkgs,skd->qkgd/dot_general | solution.py:92
  91.6 1.7 convolution_convert_fusion
  93.4 26.1 %reduce-scatter.3.cloned.1.call-done = bf16[64,2048]{1,0:T(8,128)(2,1)} async-done(((bf16[256,2048]{1,0:T(8,128)(2,1)}), bf16[64,2048]{1,0:T(8,128)(2,1)}) %reduce-scatter.3.cloned.1.call-update) | async-done | bytes 262160 | tf_op jit(solution)/shard_map/reduce_scatter | solution.py:100
  119.4 1.1 fusion.19
  120.6 1.8 fusion.21
  122.5 0.7 all-gather.8.cloned.1.call-update
  123.2 0.5 all-gather.10.cloned.1.call-update
  123.8 0.5 all-gather.12.cloned.1.call-update
  124.3 0.2 reduce-scatter.5.cloned.1.call-start
  124.5 14.7 %all-gather.6.cloned.1.call-done = bf16[256,2048]{1,0:T(8,128)(2,1)} async-done(((bf16[64,2048]{1,0:T(8,128)(2,1)}), bf16[256,2048]{1,0:T(8,128)(2,1)}) %all-gather.6.cloned.1.call-update) | async-done | bytes 1048592 | tf_op jit(solution)/shard_map/all_gather | solution.py:111
  139.3 94.5 %all-gather.8.cloned.1.call-done = bf16[2048,1408]{1,0:T(8,128)(2,1)} async-done(((bf16[256,1408]{1,0:T(8,128)(2,1)}), bf16[2048,1408]{1,0:T(8,128)(2,1)}) %all-gather.8.cloned.1.call-update) | async-done | bytes 5767184 | tf_op jit(solution)/shard_map/all_gather | solution.py:56
  233.8 5.9 %fusion.53 = f32[256,1408]{1,0:T(8,128)} fusion(bf16[256,2048]{1,0:T(8,128)(2,1)} %all-gather.6.cloned.1.call-done, bf16[2048,1408]{1,0:T(8,128)(2,1)} %all-gather.8.cloned.1.call-done), kind=kOutput, calls=%fused_computation.88 | convolution fusion | flops 1476395008 | bytes 8257536 | tf_op jit(solution)/shard_map/dot_general | solution.py:112
  239.7 86.7 %all-gather.10.cloned.1.call-done = bf16[2048,1408]{1,0:T(8,128)(2,1)} async-done(((bf16[256,1408]{1,0:T(8,128)(2,1)}), bf16[2048,1408]{1,0:T(8,128)(2,1)}) %all-gather.10.cloned.1.call-update) | async-done | bytes 5767184 | tf_op jit(solution)/shard_map/all_gather | solution.py:57
  326.3 93.2 %all-gather.12.cloned.1.call-done = bf16[1408,2048]{1,0:T(8,128)(2,1)} async-done(((bf16[1408,256]{1,0:T(8,128)(2,1)}), bf16[1408,2048]{1,0:T(8,128)(2,1)}) %all-gather.12.cloned.1.call-update) | async-done | bytes 5767184 | tf_op jit(solution)/shard_map/all_gather | solution.py:59
  419.6 9.5 %convolution_convert_fusion.1 = bf16[256,2048]{1,0:T(8,128)(2,1)} fusion(bf16[1408,2048]{1,0:T(8,128)(2,1)} %all-gather.12.cloned.1.call-done, bf16[256,2048]{1,0:T(8,128)(2,1)} %all-gather.6.cloned.1.call-done, bf16[2048,1408]{1,0:T(8,128)(2,1)} %all-gather.10.cloned.1.call-done, f32[256,1408]{1,0:T(8,128)} %fusion.53), kind=kOutput, calls=%fused_computation.10 | convolution fusion | flops 2955476992 | bytes 15073280 | tf_op jit(solution)/shard_map/dot_general | solution.py:115
  429.1 23.1 %reduce-scatter.5.cloned.1.call-done = bf16[64,2048]{1,0:T(8,128)(2,1)} async-done(((bf16[256,2048]{1,0:T(8,128)(2,1)}), bf16[64,2048]{1,0:T(8,128)(2,1)}) %reduce-scatter.5.cloned.1.call-update) | async-done | bytes 262160 | tf_op jit(solution)/shard_map/reduce_scatter | solution.py:116
  452.3 1.8 fusion.22
  (30 shorter events, 0.9 us)
Async XLA Ops:
  6.5 85.0 %copy-start = (bf16[512,2048]{1,0:T(8,128)(2,1)S(1)}, bf16[512,2048]{1,0:T(8,128)(2,1)}, u32[]{:S(2)}) copy-start(bf16[512,2048]{1,0:T(8,128)(2,1)} %param.17) | copy-start | bytes 6291460
  6.5 112.9 %reduce-scatter.3.cloned.1.call-start = ((), (), s32[]{:S(2)}) async-start(), calls=%async_computation.2 | async-start | bytes 1310720 | tf_op jit(solution)/shard_map/reduce_scatter | solution.py:100
  50.5 3.2 copy-start.1
  50.5 4.6 %copy-start.4 = (bf16[256,128]{1,0:T(8,128)(2,1)S(1)}, bf16[256,128]{1,0:T(8,128)(2,1)}, u32[]{:S(2)}) copy-start(bf16[256,128]{1,0:T(8,128)(2,1)} %param.14) | copy-start | bytes 196612
  86.5 32.9 %copy-start.2 = (bf16[64,2048]{1,0:T(8,128)(2,1)S(1)}, bf16[64,2048]{1,0:T(8,128)(2,1)}, u32[]{:S(2)}) copy-start(bf16[64,2048]{1,0:T(8,128)(2,1)} %param.11) | copy-start | bytes 786436
  86.5 34.1 %copy-start.5 = (f32[2048]{0:T(1024)S(1)}, f32[2048]{0:T(1024)}, u32[]{:S(2)}) copy-start(f32[2048]{0:T(1024)} %param.18) | copy-start | bytes 24580
  93.3 45.9 %all-gather.6.cloned.1.call-start = ((), (), s32[]{:S(2)}) async-start(), calls=%async_computation.3 | async-start | bytes 1310720 | tf_op jit(solution)/shard_map/all_gather | solution.py:111
  122.4 111.4 %all-gather.8.cloned.1.call-start = ((), (), s32[]{:S(2)}) async-start(), calls=%async_computation.4 | async-start | bytes 6488064 | tf_op jit(solution)/shard_map/all_gather | solution.py:56
  123.1 203.2 %all-gather.10.cloned.1.call-start = ((), (), s32[]{:S(2)}) async-start(), calls=%async_computation.5 | async-start | bytes 6488064 | tf_op jit(solution)/shard_map/all_gather | solution.py:57
  123.7 295.9 %all-gather.12.cloned.1.call-start = ((), (), s32[]{:S(2)}) async-start(), calls=%async_computation.6 | async-start | bytes 6488064 | tf_op jit(solution)/shard_map/all_gather | solution.py:59
  124.3 327.9 %reduce-scatter.5.cloned.1.call-start = ((), (), s32[]{:S(2)}) async-start(), calls=%async_computation.7 | async-start | bytes 1310720 | tf_op jit(solution)/shard_map/reduce_scatter | solution.py:116
  239.7 212.6 %copy-start.3 = (bf16[64,2048]{1,0:T(8,128)(2,1)S(1)}, bf16[64,2048]{1,0:T(8,128)(2,1)}, u32[]{:S(2)}) copy-start(bf16[64,2048]{1,0:T(8,128)(2,1)} %reduce-scatter.3.cloned.1.call-done) | copy-start | bytes 786436
Sparse Core Ops, SparseCore 0:
  93.4 25.9 reduce-scatter.2
  122.5 16.6 all-gather.5
  141.4 92.2 all-gather.7
  235.8 90.4 all-gather.9
  328.2 91.2 all-gather.11
  429.2 22.9 reduce-scatter.4
where the time goes:
time: 461 us
  waiting for transfers between devices  340 us (74%)
  blocking collectives  64.3 us (14%)
  matrix products  23.5 us (5%)
  other arithmetic  14.3 us (3%)
  between operations  13.6 us (3%)
    all_gather x1, waiting for transfers between devices, per_device(): lax.all_gather(gate_weight, 'sp', axis=0, tiled=True)  94.5 us
    all_gather x1, waiting for transfers between devices, per_device(): down_full = lax.all_gather(down_weight, 'sp', axis=1, tiled=True)  93.2 us
    all_gather x1, waiting for transfers between devices, per_device(): lax.all_gather(up_weight, 'sp', axis=0, tiled=True)  86.7 us
    all_gather x1, blocking collectives, per_device(): k_piece = lax.all_gather(k_rot, 'sp', axis=0, tiled=True)  33 us
    all_gather x1, blocking collectives, per_device(): v_piece = lax.all_gather(vals, 'sp', axis=0, tiled=True)  31.3 us
    reduce_scatter x1, waiting for transfers between devices, per_device(): lax.psum_scatter(jnp.dot(attended, out_weight, preferred_element_type=jnp...  26.1 us
    reduce_scatter x1, waiting for transfers between devices, per_device(): lax.psum_scatter(terms.astype(jnp.bfloat16), 'tp', scatter_dimension=0, t...  23.1 us
    all_gather x1, waiting for transfers between devices, per_device(): whole_rows = lax.all_gather(normed, 'tp', axis=0, tiled=True)  14.7 us
  transfers between devices with their start and end apart: 6, of which 6 were waited for; matrix products, arithmetic and copies ran while one was open for 1% of the time, Pallas kernels for 0%

commit v1 on v0

--- a/solution.py
+++ b/solution.py
@@ -6,6 +6,17 @@
 GRID_W = 64
 EPS = 1e-06
 THETA = 10000.0
+
+
+def pass_along(value, axis, dim):
+    devices = lax.axis_size(axis)
+    forward = [(i, (i + 1) % devices) for i in range(devices)]
+    parts = [value]
+    for far in range(1, devices):
+        parts = [lax.ppermute(parts[0], axis, forward), *parts]
+    out = jnp.concatenate(parts, axis=dim)
+    places = (lax.axis_index(axis) + 1) * parts[-1].shape[dim]
+    return jnp.roll(out, places, axis=dim)
 
 
 def turn_half(part, angles):
@@ -70,7 +81,7 @@
     )
     carry = start_state
     k_piece = lax.all_gather(k_rot, "sp", axis=0, tiled=True)
-    v_piece = lax.all_gather(vals, "sp", axis=0, tiled=True)
+    v_piece = pass_along(vals, "sp", 0)
     length = k_piece.shape[0]
     shards = length // tok
     per_step = max(1, 2048 // tok)

time: 461 us -> 457 us (level)
  blocking collectives: 64.3 us -> 31.5 us
  waiting for transfers between devices: 340 us -> 364 us
  starting transfers between devices: 0.38 us -> 6.83 us
    all_gather x1 -> x0, blocking collectives: 31.3 us -> none  [per_device(): v_piece = lax.all_gather(vals, 'sp', axis=0, tiled=True)]
    ppermute x0 -> x7, waiting for transfers between devices: none -> 27.5 us  [pass_along(): parts = [lax.ppermute(parts[0], axis, forward), *parts]]
    ppermute x0 -> x7, starting transfers between devices: none -> 6.45 us  [pass_along(): parts = [lax.ppermute(parts[0], axis, forward), *parts]]
    all_gather x1, waiting for transfers between devices: 86.7 us -> 92.6 us  [per_device(): lax.all_gather(up_weight, 'sp', axis=0, tiled=True)]
    all_gather x1, waiting for transfers between devices: 93.2 us -> 87.3 us  [per_device(): down_full = lax.all_gather(down_weight, 'sp', axis=1, tiled=True)]
  transfers between devices with their start and end apart: 6 -> 13, of which waited for: 6 -> 11; matrix products, arithmetic and copies ran while one was open for 1% -> 4% of each run, Pallas kernels for 0% -> 0%
where the time goes in v1:
time: 457 us
  waiting for transfers between devices  364 us (80%)
  blocking collectives  31.5 us (7%)
  matrix products  23.6 us (5%)
  other arithmetic  14.1 us (3%)
  between operations  13.7 us (3%)
  starting transfers between devices  6.83 us (1%)
    all_gather x1, waiting for transfers between devices, per_device(): lax.all_gather(gate_weight, 'sp', axis=0, tiled=True)  94.5 us
    all_gather x1, waiting for transfers between devices, per_device(): lax.all_gather(up_weight, 'sp', axis=0, tiled=True)  92.6 us
    all_gather x1, waiting for transfers between devices, per_device(): down_full = lax.all_gather(down_weight, 'sp', axis=1, tiled=True)  87.3 us
    all_gather x1, blocking collectives, per_device(): k_piece = lax.all_gather(k_rot, 'sp', axis=0, tiled=True)  31.5 us
    ppermute x7, waiting for transfers between devices, pass_along(): parts = [lax.ppermute(parts[0], axis, forward), *parts]  27.5 us
    reduce_scatter x1, waiting for transfers between devices, per_device(): lax.psum_scatter(terms.astype(jnp.bfloat16), 'tp', scatter_dimension=0, t...  23.2 us
    reduce_scatter x1, waiting for transfers between devices, per_device(): lax.psum_scatter(jnp.dot(attended, out_weight, preferred_element_type=jnp...  22.2 us
    all_gather x1, waiting for transfers between devices, per_device(): whole_rows = lax.all_gather(normed, 'tp', axis=0, tiled=True)  14.7 us
  transfers between devices with their start and end apart: 13, of which 11 were waited for; matrix products, arithmetic and copies ran while one was open for 4% of the time, Pallas kernels for 0%

profile of v1, /device:TPU:0, one launch (start us, length us, event | category | flops | bytes accessed | tf_op | source)
XLA Modules:
  0.0 456.7 jit_solution(4861307536852972098)
XLA Ops:
  6.5 3.0 collective-permute-start
  9.5 1.0 fusion.34
  11.2 1.2 fusion.42
  12.4 1.1 copy.14
  13.7 0.9 multiply_multiply_fusion
  15.1 0.9 fusion.36
  16.0 1.4 fusion.26
  17.6 1.6 collective-permute-start.1
  19.2 1.2 fusion.40
  20.4 4.4 collective-permute-done.1
  24.9 6.9 %collective-permute-done.2 = bf16[256,1,128]{2,0,1:T(8,128)(2,1)S(1)} collective-permute-done((bf16[256,1,128]{2,0,1:T(8,128)(2,1)S(1)}, bf16[256,1,128]{2,0,1:T(8,128)(2,1)S(1)}, u32[]{:S(2)}, u32[]{:S(2)}) %collective-permute-start.2) | collective-permute-done | bytes 65568 | tf_op jit(solution)/shard_map/ppermute | solution.py:16
  31.8 31.5 %all_gather.15 = bf16[2048,1,128]{2,0,1:T(8,128)(2,1)S(1)} all-gather(bf16[256,1,128]{2,0,1:T(8,128)(2,1)S(1)} %pad_maximum_fusion.4), channel_id=1, replica_groups=mesh['sp'=8,'tp'=4] {'sp'}, dimensions={0}, use_global_device_ids=true | all-gather | bytes 589824 | tf_op jit(solution)/shard_map/all_gather | solution.py:83
  63.3 1.9 collective-permute-start.4
  65.2 1.3 bitcast_reduce_fusion
  66.5 3.7 collective-permute-done.4
  70.2 1.4 fusion.1
  71.6 5.6 %collective-permute-done.5 = bf16[256,1,128]{2,0,1:T(8,128)(2,1)S(1)} collective-permute-done((bf16[256,1,128]{2,0,1:T(8,128)(2,1)S(1)}, bf16[256,1,128]{2,0,1:T(8,128)(2,1)S(1)}, u32[]{:S(2)}, u32[]{:S(2)}) %collective-permute-start.5) | collective-permute-done | bytes 65568 | tf_op jit(solution)/shard_map/ppermute | solution.py:16
  77.2 6.9 %collective-permute-done.6 = bf16[256,1,128]{2,0,1:T(8,128)(2,1)S(1)} collective-permute-done((bf16[256,1,128]{2,0,1:T(8,128)(2,1)S(1)}, bf16[256,1,128]{2,0,1:T(8,128)(2,1)S(1)}, u32[]{:S(2)}, u32[]{:S(2)}) %collective-permute-start.6) | collective-permute-done | bytes 65568 | tf_op jit(solution)/shard_map/ppermute | solution.py:16
  84.3 0.9 constant_dynamic-update-slice_fusion.9
  86.2 5.1 %fusion.16 = bf16[1,128,256,4]{2,1,3,0:T(8,128)(2,1)S(1)} fusion(f32[2048,256,4]{1,0,2:T(8,128)} %copy-done.1, f32[256,4]{0,1:T(4,128)S(1)} %get-tuple-element.50, bf16[4096,1,128]{2,0,1:T(8,128)(2,1)S(1)} %constant_dynamic-update-slice_fusion, s32[]{:T(128)S(6)} %select_n.38, f32[256,4]{0,1:T(4,128)S(1)} %get-tuple-element.43, ...), kind=kOutput, calls=%fused_computation.14 | convolution fusion | flops 543555584 | bytes 9187332 | tf_op jit(solution)/shard_map/while/body/eval_jaxpr/qkgs,skd->qkgd/dot_general | solution.py:103
  91.3 1.7 convolution_convert_fusion
  93.1 22.2 %reduce-scatter.3.cloned.1.call-done = bf16[64,2048]{1,0:T(8,128)(2,1)} async-done(((bf16[256,2048]{1,0:T(8,128)(2,1)}), bf16[64,2048]{1,0:T(8,128)(2,1)}) %reduce-scatter.3.cloned.1.call-update) | async-done | bytes 262160 | tf_op jit(solution)/shard_map/reduce_scatter | solution.py:111
  115.3 1.1 fusion.19
  116.5 1.8 fusion.21
  120.4 14.7 %all-gather.5.cloned.1.call-done = bf16[256,2048]{1,0:T(8,128)(2,1)} async-done(((bf16[64,2048]{1,0:T(8,128)(2,1)}), bf16[256,2048]{1,0:T(8,128)(2,1)}) %all-gather.5.cloned.1.call-update) | async-done | bytes 1048592 | tf_op jit(solution)/shard_map/all_gather | solution.py:122
  135.1 94.5 %all-gather.7.cloned.1.call-done = bf16[2048,1408]{1,0:T(8,128)(2,1)} async-done(((bf16[256,1408]{1,0:T(8,128)(2,1)}), bf16[2048,1408]{1,0:T(8,128)(2,1)}) %all-gather.7.cloned.1.call-update) | async-done | bytes 5767184 | tf_op jit(solution)/shard_map/all_gather | solution.py:67
  229.6 5.9 %fusion.55 = f32[256,1408]{1,0:T(8,128)} fusion(bf16[256,2048]{1,0:T(8,128)(2,1)} %all-gather.5.cloned.1.call-done, bf16[2048,1408]{1,0:T(8,128)(2,1)} %all-gather.7.cloned.1.call-done), kind=kOutput, calls=%fused_computation.106 | convolution fusion | flops 1476395008 | bytes 8257536 | tf_op jit(solution)/shard_map/dot_general | solution.py:123
  235.5 87.3 %all-gather.11.cloned.1.call-done = bf16[1408,2048]{1,0:T(8,128)(2,1)} async-done(((bf16[1408,256]{1,0:T(8,128)(2,1)}), bf16[1408,2048]{1,0:T(8,128)(2,1)}) %all-gather.11.cloned.1.call-update) | async-done | bytes 5767184 | tf_op jit(solution)/shard_map/all_gather | solution.py:70
  322.9 92.6 %all-gather.9.cloned.1.call-done = bf16[2048,1408]{1,0:T(8,128)(2,1)} async-done(((bf16[256,1408]{1,0:T(8,128)(2,1)}), bf16[2048,1408]{1,0:T(8,128)(2,1)}) %all-gather.9.cloned.1.call-update) | async-done | bytes 5767184 | tf_op jit(solution)/shard_map/all_gather | solution.py:68
  415.4 9.5 %convolution_convert_fusion.1 = bf16[256,2048]{1,0:T(8,128)(2,1)} fusion(bf16[1408,2048]{1,0:T(8,128)(2,1)} %all-gather.11.cloned.1.call-done, bf16[256,2048]{1,0:T(8,128)(2,1)} %all-gather.5.cloned.1.call-done, bf16[2048,1408]{1,0:T(8,128)(2,1)} %all-gather.9.cloned.1.call-done, f32[256,1408]{1,0:T(8,128)} %fusion.55), kind=kOutput, calls=%fused_computation.10 | convolution fusion | flops 2955476992 | bytes 15073280 | tf_op jit(solution)/shard_map/dot_general | solution.py:126
  425.0 23.2 %reduce-scatter.5.cloned.1.call-done = bf16[64,2048]{1,0:T(8,128)(2,1)} async-done(((bf16[256,2048]{1,0:T(8,128)(2,1)}), bf16[64,2048]{1,0:T(8,128)(2,1)}) %reduce-scatter.5.cloned.1.call-update) | async-done | bytes 262160 | tf_op jit(solution)/shard_map/reduce_scatter | solution.py:127
  448.1 1.8 fusion.22
  (60 shorter events, 4.9 us)
Async XLA Ops:
  6.5 84.7 %copy-start = (bf16[512,2048]{1,0:T(8,128)(2,1)S(1)}, bf16[512,2048]{1,0:T(8,128)(2,1)}, u32[]{:S(2)}) copy-start(bf16[512,2048]{1,0:T(8,128)(2,1)} %param.17) | copy-start | bytes 6291460
  6.5 8.5 %copy-start.6 = (f32[128]{0:T(128)S(1)}, f32[128]{0:T(128)}, u32[]{:S(2)}) copy-start(f32[128]{0:T(128)} %param.16) | copy-start | bytes 1540
  6.5 108.7 %reduce-scatter.3.cloned.1.call-start = ((), (), s32[]{:S(2)}) async-start(), calls=%async_computation.2 | async-start | bytes 1310720 | tf_op jit(solution)/shard_map/reduce_scatter | solution.py:111
  6.5 11.0 %collective-permute-start = (bf16[256,1,128]{2,0,1:T(8,128)(2,1)}, bf16[256,1,128]{2,0,1:T(8,128)(2,1)}, u32[]{:S(2)}, u32[]{:S(2)}) collective-permute-start(bf16[256,1,128]{2,0,1:T(8,128)(2,1)} %bitcast.76), channel_id=1, source_target_pairs={{0,4},{4,8},{8,12},{12,16},{16,20},{20,24},{24,28},{28,0},{1,5},{5... | collective-permute-start | bytes 196616 | tf_op jit(solution)/shard_map/ppermute | solution.py:16
  17.6 7.2 %collective-permute-start.1 = (bf16[256,1,128]{2,0,1:T(8,128)(2,1)}, bf16[256,1,128]{2,0,1:T(8,128)(2,1)S(1)}, u32[]{:S(2)}, u32[]{:S(2)}) collective-permute-start(bf16[256,1,128]{2,0,1:T(8,128)(2,1)} %collective-permute-done), channel_id=1, source_target_pairs={{0,4},{4,8},{8,12},{12,16},{16,20},{20,24},{24,28},{28,0},{1,5},{5... | collective-permute-start | bytes 196616 | tf_op jit(solution)/shard_map/ppermute | solution.py:16
  24.8 7.0 %collective-permute-start.2 = (bf16[256,1,128]{2,0,1:T(8,128)(2,1)S(1)}, bf16[256,1,128]{2,0,1:T(8,128)(2,1)S(1)}, u32[]{:S(2)}, u32[]{:S(2)}) collective-permute-start(bf16[256,1,128]{2,0,1:T(8,128)(2,1)S(1)} %collective-permute-done.1), channel_id=1, source_target_pairs={{0,4},{4,8},{8,12},{12,16},{16,20},{20,24},{24,28},{28,0},{1,5},{5... | collective-permute-start | bytes 196616 | tf_op jit(solution)/shard_map/ppermute | solution.py:16
  31.8 31.5 %collective-permute-start.3 = (bf16[256,1,128]{2,0,1:T(8,128)(2,1)S(1)}, bf16[256,1,128]{2,0,1:T(8,128)(2,1)S(1)}, u32[]{:S(2)}, u32[]{:S(2)}) collective-permute-start(bf16[256,1,128]{2,0,1:T(8,128)(2,1)S(1)} %collective-permute-done.2), channel_id=1, source_target_pairs={{0,4},{4,8},{8,12},{12,16},{16,20},{20,24},{24,28},{28,0},{1,5},{5... | collective-permute-start | bytes 196616 | tf_op jit(solution)/shard_map/ppermute | solution.py:16
  63.3 7.0 %collective-permute-start.4 = (bf16[256,1,128]{2,0,1:T(8,128)(2,1)S(1)}, bf16[256,1,128]{2,0,1:T(8,128)(2,1)S(1)}, u32[]{:S(2)}, u32[]{:S(2)}) collective-permute-start(bf16[256,1,128]{2,0,1:T(8,128)(2,1)S(1)} %collective-permute-done.3), channel_id=1, source_target_pairs={{0,4},{4,8},{8,12},{12,16},{16,20},{20,24},{24,28},{28,0},{1,5},{5... | collective-permute-start | bytes 196616 | tf_op jit(solution)/shard_map/ppermute | solution.py:16
  66.5 3.8 copy-start.1
  66.5 18.6 %copy-start.4 = (bf16[256,128]{1,0:T(8,128)(2,1)S(1)}, bf16[256,128]{1,0:T(8,128)(2,1)}, u32[]{:S(2)}) copy-start(bf16[256,128]{1,0:T(8,128)(2,1)} %param.14) | copy-start | bytes 196612
  70.2 7.0 %collective-permute-start.5 = (bf16[256,1,128]{2,0,1:T(8,128)(2,1)S(1)}, bf16[256,1,128]{2,0,1:T(8,128)(2,1)S(1)}, u32[]{:S(2)}, u32[]{:S(2)}) collective-permute-start(bf16[256,1,128]{2,0,1:T(8,128)(2,1)S(1)} %collective-permute-done.4), channel_id=1, source_target_pairs={{0,4},{4,8},{8,12},{12,16},{16,20},{20,24},{24,28},{28,0},{1,5},{5... | collective-permute-start | bytes 196616 | tf_op jit(solution)/shard_map/ppermute | solution.py:16
  77.2 7.0 %collective-permute-start.6 = (bf16[256,1,128]{2,0,1:T(8,128)(2,1)S(1)}, bf16[256,1,128]{2,0,1:T(8,128)(2,1)S(1)}, u32[]{:S(2)}, u32[]{:S(2)}) collective-permute-start(bf16[256,1,128]{2,0,1:T(8,128)(2,1)S(1)} %collective-permute-done.5), channel_id=1, source_target_pairs={{0,4},{4,8},{8,12},{12,16},{16,20},{20,24},{24,28},{28,0},{1,5},{5... | collective-permute-start | bytes 196616 | tf_op jit(solution)/shard_map/ppermute | solution.py:16
  86.1 29.2 %copy-start.2 = (bf16[64,2048]{1,0:T(8,128)(2,1)S(1)}, bf16[64,2048]{1,0:T(8,128)(2,1)}, u32[]{:S(2)}) copy-start(bf16[64,2048]{1,0:T(8,128)(2,1)} %param.11) | copy-start | bytes 786436
  86.1 30.3 %copy-start.5 = (f32[2048]{0:T(1024)S(1)}, f32[2048]{0:T(1024)}, u32[]{:S(2)}) copy-start(f32[2048]{0:T(1024)} %param.18) | copy-start | bytes 24580
  93.0 42.1 %all-gather.5.cloned.1.call-start = ((), (), s32[]{:S(2)}) async-start(), calls=%async_computation.3 | async-start | bytes 1310720 | tf_op jit(solution)/shard_map/all_gather | solution.py:122
  118.2 111.4 %all-gather.7.cloned.1.call-start = ((), (), s32[]{:S(2)}) async-start(), calls=%async_computation.4 | async-start | bytes 6488064 | tf_op jit(solution)/shard_map/all_gather | solution.py:67
  119.0 203.9 %all-gather.11.cloned.1.call-start = ((), (), s32[]{:S(2)}) async-start(), calls=%async_computation.6 | async-start | bytes 6488064 | tf_op jit(solution)/shard_map/all_gather | solution.py:70
  119.6 295.9 %all-gather.9.cloned.1.call-start = ((), (), s32[]{:S(2)}) async-start(), calls=%async_computation.5 | async-start | bytes 6488064 | tf_op jit(solution)/shard_map/all_gather | solution.py:68
  120.1 328.0 %reduce-scatter.5.cloned.1.call-start = ((), (), s32[]{:S(2)}) async-start(), calls=%async_computation.7 | async-start | bytes 1310720 | tf_op jit(solution)/shard_map/reduce_scatter | solution.py:127
  235.5 212.6 %copy-start.3 = (bf16[64,2048]{1,0:T(8,128)(2,1)S(1)}, bf16[64,2048]{1,0:T(8,128)(2,1)}, u32[]{:S(2)}) copy-start(bf16[64,2048]{1,0:T(8,128)(2,1)} %reduce-scatter.3.cloned.1.call-done) | copy-start | bytes 786436
Sparse Core Ops, SparseCore 0:
  93.2 22.0 reduce-scatter.2
  118.4 16.6 all-gather.4
  137.3 92.2 all-gather.6
  231.5 91.3 all-gather.10
  324.9 90.4 all-gather.8
  425.1 22.9 reduce-scatter.4
